TPU v7x, 32 devices: a whole 2x2x4 slice. The times are simulated.
32 devices in a mesh: dp: 4 (over y, x), kv: 4 (over z), tp: 2 (over core).
Axes of the slice: x: 2, y: 2, z: 4, core: 2. Of those that a mesh axis runs over, the one named last changes fastest.
Arguments:
- tokens: bfloat16 [16, 4096], P('dp', ('kv', 'tp')), may hold values from -11 to 11
- attn_gain: float32 [4096], replicated, may hold values from 0.1 to 1.9
- query_weight: bfloat16 [4096, 4096], P('kv', 'tp'), may hold values from -0.09375 to 0.09375
- key_cache: bfloat16 [16, 1024, 2, 128], P('dp', 'kv', 'tp'), may hold values from -820 to 820
- value_cache: bfloat16 [16, 1024, 2, 128], P('dp', 'kv', 'tp'), may hold values from -6 to 6
- head_lambda: float32 [32], P('tp'), may hold values from 0.3 to 0.8
- head_gain: float32 [128], replicated, may hold values from 0.1 to 1.9
- out_weight: bfloat16 [4096, 4096], P('kv', 'tp'), may hold values from -0.09375 to 0.09375
- mlp_gain: float32 [4096], replicated, may hold values from 0.1 to 1.9
- gate_weight: bfloat16 [11264, 4096], P(('kv', 'tp')), may hold values from -0.09375 to 0.09375
- up_weight: bfloat16 [11264, 4096], P(('kv', 'tp')), may hold values from -0.09375 to 0.09375
- down_weight: bfloat16 [11264, 4096], P(('kv', 'tp')), may hold values from -0.078125 to 0.078125
Outputs:
- mixed: bfloat16 [16, 4096], P('dp', ('kv', 'tp'))
All inputs are finite; a program needn't handle non-finite values.
Results may differ from a plain program's by a relative error of at most 0.02.
The roundings to bfloat16 on the way count: a program that leaves them out, or rounds other values in their place, can miss the bound.
Values may be sent and summed in bfloat16 or wider, within the bound.
A program may use at most 128 MiB of HBM per device.

v0:
```python
import functools

import jax
import jax.numpy as jnp
import numpy as np
from jax import lax
from jax.experimental import pallas as pl
from jax.experimental.pallas import tpu as pltpu
from jax.sharding import PartitionSpec as P

EPS = 1e-06
THETA = 10000.0
LANES = 128
CUTS = (5, 13, 22)


def merged(x, axis, combine):
    everything = jax.tree.map(lambda part: lax.all_gather(part, axis), x)
    first = jax.tree.map(lambda part: part[0], everything)

    def hop(k, so_far):
        return combine(so_far, jax.tree.map(lambda part: part[k], everything))

    return lax.fori_loop(1, lax.axis_size(axis), hop, first)


def rotate(vector, position):
    half_len = vector.shape[-1] // 2
    inv_freq = 1.0 / THETA ** (jnp.arange(half_len, dtype=jnp.float32) / half_len)
    angles = position * inv_freq
    cos_table = jnp.cos(angles)
    sin_table = jnp.sin(angles)
    first_half = vector[..., :half_len]
    second_half = vector[..., half_len:]
    return jnp.concatenate(
        [
            first_half * cos_table - second_half * sin_table,
            second_half * cos_table + first_half * sin_table,
        ],
        axis=-1,
    )


def combine(earlier, latter):
    peak_a, total_a, value_a = earlier
    peak_b, total_b, value_b = latter
    peak_new = jnp.maximum(peak_a, peak_b)
    factor_a = jnp.exp(peak_a - peak_new)
    factor_b = jnp.exp(peak_b - peak_new)
    return (
        peak_new,
        total_a * factor_a + total_b * factor_b,
        value_a * factor_a[..., None] + value_b * factor_b[..., None],
    )


def inner_last(left, right):
    return lax.dot_general(
        left, right, (((1,), (1,)), ((), ())), preferred_element_type=jnp.float32
    )


def shards(
    tokens,
    attn_gain,
    query_weight,
    key_cache,
    value_cache,
    head_lambda,
    head_gain,
    out_weight,
    mlp_gain,
    gate_weight,
    up_weight,
    down_weight,
):
    row_count = tokens.shape[0]
    kv_count = lax.axis_size("kv")
    tp_count = lax.axis_size("tp")
    kv_index = lax.axis_index("kv")
    row_span = query_weight.shape[0]
    full_rows = lax.all_gather(tokens, ("kv", "tp"), axis=1, tiled=True)
    wide_rows = full_rows.astype(jnp.float32)
    mean_square = jnp.mean(wide_rows * wide_rows, axis=-1, keepdims=True)
    scaled = (wide_rows * attn_gain).astype(jnp.bfloat16)
    local_cols = lax.dynamic_slice_in_dim(scaled, kv_index * row_span, row_span, 1)
    queries = lax.psum(jnp.dot(local_cols, query_weight, preferred_element_type=jnp.float32), "kv")
    queries = queries * lax.rsqrt(mean_square + EPS)
    head_count = head_lambda.shape[0]
    kv_local = key_cache.shape[2]
    group_size = head_count // kv_local
    position_count = key_cache.shape[1]
    half_dim = key_cache.shape[3] // 2
    value_dim = value_cache.shape[3]
    queries = queries.reshape(row_count, kv_local, group_size, 2, half_dim)
    rotated = rotate(queries, jnp.float32(position_count * kv_count)).astype(jnp.bfloat16)
    key_grid = key_cache.reshape(row_count, position_count, kv_local, 2, half_dim)
    scores = jnp.einsum(
        "bkgch,bpkch->bkgcp", rotated, key_grid, preferred_element_type=jnp.float32
    ) * half_dim ** (-0.5)
    local_peak = jnp.max(scores, axis=-1)
    weights_exp = jnp.exp(scores - local_peak[..., None])
    lam_grid = head_lambda.reshape(kv_local, group_size)[None, :, :, None]
    exp_total = jnp.sum(weights_exp, axis=-1)
    weighted = jnp.einsum(
        "bkgcp,bpkv->bkgcv",
        weights_exp.astype(jnp.bfloat16),
        value_cache,
        preferred_element_type=jnp.float32,
    )
    peak_all, total_all, weighted_all = merged((local_peak, exp_total, weighted), "kv", combine)
    attended = weighted_all / total_all[..., None]
    difference = attended[:, :, :, 0] - lam_grid * attended[:, :, :, 1]
    head_norm = lax.rsqrt(jnp.mean(difference * difference, axis=-1, keepdims=True) + EPS)
    head_out = (difference * head_norm * head_gain).reshape(row_count, head_count * value_dim)
    head_out = head_out.astype(jnp.bfloat16)
    out_part = inner_last(head_out, out_weight).astype(jnp.bfloat16)
    pieces = lax.all_gather(out_part, ("kv", "tp"), axis=1, tiled=True)
    attention = jnp.sum(
        pieces.astype(jnp.float32).reshape(row_count, kv_count, tp_count, -1), axis=2
    )
    stream = wide_rows + attention.reshape(row_count, -1)
    stream_square = jnp.mean(stream * stream, axis=-1, keepdims=True)
    normed = (stream * lax.rsqrt(stream_square + EPS) * mlp_gain).astype(jnp.bfloat16)
    gate_out = inner_last(normed, gate_weight)
    up_out = inner_last(normed, up_weight)
    hidden = (jax.nn.silu(gate_out) * up_out).astype(jnp.bfloat16)
    own_cols = tokens.shape[1]
    down_cols = lax.psum_scatter(
        lax.dot_general(
            down_weight, hidden, (((0,), (1,)), ((), ())), preferred_element_type=jnp.float32
        ),
        ("kv", "tp"),
        scatter_dimension=0,
        tiled=True,
    )
    column_index = lax.axis_index(("kv", "tp"))
    own_stream = lax.dynamic_slice_in_dim(stream, column_index * own_cols, own_cols, 1)
    return (own_stream + down_cols.T).astype(jnp.bfloat16)


def same_chip_kernel(
    kv_n, tp_n, tok, again, wq_h, kc_h, vc_h, lam, hgain, wo_h, mgain, wg_h, wu_h, wd_h, table,
    out,
    wq, kc, vc, wo, stage, wgu_t, wd,
    tg, qs, qr, qf, ms, mb, mr, st, sr, hf, og, og_r, stream, hid, ds, dr,
    wsem, csem, tsend, trecv, qsend, qrecv, msend, mrecv, hsend, hrecv, osend, orecv, dsend, drecv,
):
    kv, tp = lax.axis_index("kv"), lax.axis_index("tp")
    n_all = kv_n * tp_n
    me = kv * tp_n + tp
    rows, own = tok.shape
    loads = []
    for slot, (src, dst) in enumerate(
        [(wq_h, wq), (kc_h, kc), (vc_h, vc), (wo_h, wo)]
    ):
        load = pltpu.make_async_copy(src, dst, wsem.at[slot])
        load.start()
        loads.append(load)
    features = wo.shape[0]
    units = wg_h.shape[0]
    per_weight = units // LANES
    chunks = 2 * per_weight
    slots = stage.shape[0]

    def chunk_load(weight, i, slot):
        piece = pl.ds(pl.multiple_of(i * LANES, LANES), LANES)
        at = i if weight is wg_h else i + per_weight
        return pltpu.make_async_copy(weight.at[piece], stage.at[slot], csem.at[at])

    for g in range(slots):
        if g < per_weight:
            chunk_load(wg_h, g, g).start()
        else:
            chunk_load(wu_h, g - per_weight, g).start()

    def turn(low, high):
        def turn_gate(i, carry):
            slot = lax.rem(i, slots)
            chunk_load(wg_h, i, slot).wait()
            at = pl.ds(pl.multiple_of(i * LANES, LANES), LANES)
            wgu_t[0, :, at] = stage[slot].T

            @pl.when(i + slots < chunks)
            def _():
                chunk_load(wu_h, i + slots - per_weight, slot).start()

            return carry

        def turn_up(i, carry):
            slot = lax.rem(i + per_weight, slots)
            chunk_load(wu_h, i, slot).wait()
            at = pl.ds(pl.multiple_of(i * LANES, LANES), LANES)
            wgu_t[1, :, at] = stage[slot].T
            return carry

        low, high = chunks * low // 22, chunks * high // 22
        if low < per_weight:
            lax.fori_loop(low, min(high, per_weight), turn_gate, 0)
        if high > per_weight:
            lax.fori_loop(max(low, per_weight) - per_weight, high - per_weight, turn_up, 0)

    down_load = pltpu.make_async_copy(wd_h, wd, wsem.at[4])
    down_load.start()

    def spot(delta):
        other = lax.rem(me + delta, n_all)
        return {"kv": other // tp_n, "tp": lax.rem(other, tp_n)}

    def along(delta):
        return {"kv": lax.rem(kv + delta, kv_n), "tp": tp}

    def remote(src, dst, send, recv, where):
        copy = pltpu.make_async_remote_copy(
            src_ref=src, dst_ref=dst, send_sem=send, recv_sem=recv,
            device_id=where, device_id_type=pl.DeviceIdType.MESH,
        )
        copy.start()
        return copy

    barrier = pltpu.get_barrier_semaphore()
    for delta in range(1, n_all):
        pl.semaphore_signal(
            barrier, inc=1, device_id=spot(delta), device_id_type=pl.DeviceIdType.MESH
        )
    tg[me] = tok[...]
    pl.semaphore_wait(barrier, n_all - 1)
    sends = []

    mate = {"kv": kv, "tp": lax.rem(tp + 1, tp_n)}
    pair = remote(tok, tg.at[me], tsend.at[0], trecv.at[0], mate)
    token_copies = [pair]
    for delta in range(1, kv_n):
        for across in range(tp_n):
            where = {"kv": lax.rem(kv + delta, kv_n), "tp": lax.rem(tp + across, tp_n)}
            slot = delta * tp_n + across
            token_copies.append(remote(tok, tg.at[me], tsend.at[slot], trecv.at[slot], where))
    sends += token_copies

    pair.wait_recv()
    parts = []
    for half in range(tp_n):
        at = kv * tp_n + half
        gain = again[:, pl.ds(pl.multiple_of(at * own, LANES), own)]
        parts.append((tg[at].astype(jnp.float32) * gain).astype(jnp.bfloat16))
    scaled = jnp.concatenate(parts, axis=1)
    loads[0].wait()
    head_count = qs.shape[0]
    value_dim = qs.shape[2]
    per = 4
    pieces = head_count // per
    query_copies = []
    for j in range(pieces):
        width = per * value_dim
        product = jnp.dot(
            scaled, wq[:, j * width:(j + 1) * width], preferred_element_type=jnp.float32
        )
        for i in range(per):
            qs[j * per + i] = product[:, i * value_dim:(i + 1) * value_dim]
        for delta in range(1, kv_n):
            part = pl.ds(j * per, per)
            query_copies.append(
                remote(
                    qs.at[part], qr.at[delta - 1, part],
                    qsend.at[j, delta - 1], qrecv.at[j, delta - 1], along(delta),
                )
            )
    sends += query_copies

    for copy in token_copies[1:]:
        copy.wait_recv()
    square = jnp.zeros((rows, 1), jnp.float32)
    for at in range(n_all):
        wide = tg[at].astype(jnp.float32)
        square = square + jnp.sum(wide * wide, axis=1, keepdims=True)
    scale = lax.rsqrt(square / (n_all * own) + EPS)

    turn(0, CUTS[0])
    for copy in query_copies:
        copy.wait_recv()
    lane = lax.broadcasted_iota(jnp.int32, (rows, value_dim), 1)
    half = value_dim // 2
    first = lax.rem(lane, half) < half // 2
    cosines = table[0:1, :]
    sines = table[1:2, :]
    for h in range(head_count):
        total = qs[h]
        for delta in range(1, kv_n):
            total = total + qr[delta - 1, h]
        total = total * scale
        swapped = jnp.where(
            first,
            pltpu.roll(total, value_dim - half // 2, 1),
            pltpu.roll(total, half // 2, 1),
        )
        qf[h] = total * cosines + swapped * sines

    loads[1].wait()
    loads[2].wait()
    both = 2 * head_count
    low = lax.broadcasted_iota(jnp.int32, (head_count, value_dim), 1) < half
    row_at = lax.broadcasted_iota(jnp.int32, (both, value_dim), 0)
    lane_at = lax.broadcasted_iota(jnp.int32, (both, value_dim), 1)
    spread = []
    for b in range(rows):
        query = qf[:, b, :]
        grid = jnp.concatenate(
            [jnp.where(low, query, 0.0), jnp.where(low, 0.0, query)], axis=0
        ).astype(jnp.bfloat16)
        scores = inner_last(grid, kc[b]) * half ** (-0.5)
        peak = jnp.max(scores, axis=1, keepdims=True)
        exps = jnp.exp(scores - peak)
        sums = jnp.sum(exps, axis=1, keepdims=True)
        spread.append(exps.astype(jnp.bfloat16))
        stats = jnp.where(lane_at == row_at, peak, 0.0) + jnp.where(
            lane_at == row_at + both, sums, 0.0
        )
        st[b:b + 1, :] = jnp.sum(stats, axis=0, keepdims=True)
    stat_copies = []
    for delta in range(1, kv_n):
        stat_copies.append(
            remote(
                st, sr.at[delta - 1], hsend.at[delta - 1], hrecv.at[delta - 1], along(delta)
            )
        )
    merge_copies = []
    for b in range(rows):
        values = jnp.dot(spread[b], vc[b], preferred_element_type=jnp.float32)
        ms[b] = values
        mb[b] = values.astype(jnp.bfloat16)
        for delta in range(1, kv_n):
            merge_copies.append(
                remote(
                    mb.at[b], mr.at[delta - 1, b],
                    msend.at[b, delta - 1], mrecv.at[b, delta - 1], along(delta),
                )
            )
    sends += stat_copies + merge_copies

    lam_at = lax.broadcasted_iota(jnp.int32, (head_count, head_count), 0)
    lam_lane = lax.broadcasted_iota(jnp.int32, (head_count, head_count), 1)
    lam_col = jnp.sum(
        jnp.where(lam_at == lam_lane, lam[...], 0.0), axis=1, keepdims=True
    )
    turn(CUTS[0], CUTS[1])
    for copy in stat_copies:
        copy.wait_recv()
    for b in range(rows):
        for copy in merge_copies[b * (kv_n - 1):(b + 1) * (kv_n - 1)]:
            copy.wait_recv()
        gathered = []
        for source in range(kv_n):
            stats = st[b:b + 1, :] if source == 0 else sr[source - 1, b:b + 1, :]
            values = ms[b] if source == 0 else mr[source - 1, b].astype(jnp.float32)
            peak = jnp.sum(jnp.where(lane_at == row_at, stats, 0.0), axis=1, keepdims=True)
            sums = jnp.sum(
                jnp.where(lane_at == row_at + both, stats, 0.0), axis=1, keepdims=True
            )
            gathered.append((peak, sums, values))
        top = gathered[0][0]
        for peak, _, _ in gathered[1:]:
            top = jnp.maximum(top, peak)
        all_sums = jnp.zeros_like(top)
        weighted = jnp.zeros((both, value_dim), jnp.float32)
        for peak, sums, values in gathered:
            factor = jnp.exp(peak - top)
            all_sums = all_sums + sums * factor
            weighted = weighted + values * factor
        attended = weighted / all_sums
        difference = attended[0:head_count] - lam_col * attended[head_count:both]
        norm = lax.rsqrt(jnp.mean(difference * difference, axis=1, keepdims=True) + EPS)
        hf[b] = difference * norm * hgain[...]
    flat = jnp.concatenate(
        [hf[:, h, :] for h in range(head_count)], axis=1
    ).astype(jnp.bfloat16)
    loads[3].wait()
    width = 256
    for j in range(features // width):
        part = inner_last(flat, wo[j * width:(j + 1) * width, :]).astype(jnp.bfloat16)
        og[:, j * width:(j + 1) * width] = part
    og_r[me] = og[...]
    out_copies = []
    for delta in range(1, n_all):
        out_copies.append(
            remote(og, og_r.at[me], osend.at[delta - 1], orecv.at[delta - 1], spot(delta))
        )
    sends += out_copies
    turn(CUTS[1], CUTS[2])
    for copy in out_copies:
        copy.wait_recv()
    square = jnp.zeros((rows, 1), jnp.float32)
    for at in range(kv_n):
        tokens = jnp.concatenate(
            [tg[at * tp_n + g].astype(jnp.float32) for g in range(tp_n)], axis=1
        )
        attention = og_r[at * tp_n].astype(jnp.float32)
        for g in range(1, tp_n):
            attention = attention + og_r[at * tp_n + g].astype(jnp.float32)
        piece = tokens + attention
        stream[:, at * features:(at + 1) * features] = piece
        square = square + jnp.sum(piece * piece, axis=1, keepdims=True)
    scale = lax.rsqrt(square / (n_all * own) + EPS)
    normed = (stream[...] * scale * mgain[...]).astype(jnp.bfloat16)

    step = 2 * LANES
    for low in range(0, units, step):
        at = slice(low, min(low + step, units))
        gate = jnp.dot(normed, wgu_t[0, :, at], preferred_element_type=jnp.float32)
        up = jnp.dot(normed, wgu_t[1, :, at], preferred_element_type=jnp.float32)
        hid[:, at] = (gate / (1.0 + jnp.exp(-gate)) * up).astype(jnp.bfloat16)
    hidden = hid[...]
    down_load.wait()
    order = [n_all // 2 + (i + 1) // 2 * (1 if i % 2 else -1) for i in range(n_all)]
    order = [d for d in order if 0 < d < n_all] + [0]
    down_copies = []
    mine = None
    for delta in order:
        at = lax.rem(me + delta, n_all)
        block = jnp.dot(
            hidden,
            wd[:, pl.ds(pl.multiple_of(at * own, LANES), own)],
            preferred_element_type=jnp.float32,
        )
        if delta == 0:
            mine = block
        else:
            ds[delta - 1] = block.astype(ds.dtype)
            down_copies.append(
                remote(
                    ds.at[delta - 1], dr.at[delta - 1],
                    dsend.at[delta - 1], drecv.at[delta - 1], spot(delta),
                )
            )
    sends += down_copies
    total = mine
    for copy in down_copies:
        copy.wait_recv()
    for delta in range(1, n_all):
        total = total + dr[delta - 1].astype(jnp.float32)
    mixed = stream[:, pl.ds(pl.multiple_of(me * own, LANES), own)] + total
    out[...] = mixed.astype(out.dtype)
    for copy in sends:
        copy.wait_send()


def turning(head_dim, position):
    half_len = head_dim // 4
    inv_freq = np.float32(1.0) / np.float32(THETA) ** (
        np.arange(half_len, dtype=np.float32) / np.float32(half_len)
    )
    angles = (np.float32(position) * inv_freq.astype(np.float32)).astype(np.float32)
    cos, sin = np.cos(angles), np.sin(angles)
    return np.stack(
        [np.concatenate([cos, cos] * 2), np.concatenate([-sin, sin] * 2)]
    ).astype(np.float32)


def fused(kv_n, tp_n, *arrays):
    (tokens, attn_gain, wq, kc, vc, lam, hgain, wo, mgain, wg, wu, wd) = arrays
    rows, own = tokens.shape
    n_all = kv_n * tp_n
    positions, value_dim = kc.shape[1], kc.shape[3]
    heads = lam.shape[0]
    both = 2 * heads
    model = n_all * own
    per_weight = wg.shape[0] // LANES
    f32, bf16 = jnp.float32, jnp.bfloat16
    table = jnp.asarray(turning(value_dim, positions * kv_n))
    dma = pltpu.SemaphoreType.DMA
    vmem = pl.BlockSpec(memory_space=pltpu.VMEM)
    hbm = pl.BlockSpec(memory_space=pl.ANY)
    return pl.pallas_call(
        functools.partial(same_chip_kernel, kv_n, tp_n),
        out_shape=jax.ShapeDtypeStruct((rows, own), tokens.dtype),
        in_specs=[vmem, vmem, hbm, hbm, hbm, vmem, vmem, hbm, vmem, hbm, hbm, hbm, vmem],
        out_specs=vmem,
        scratch_shapes=[
            pltpu.VMEM(wq.shape, bf16),
            pltpu.VMEM((rows, positions, value_dim), bf16),
            pltpu.VMEM((rows, positions, value_dim), bf16),
            pltpu.VMEM(wo.shape, bf16),
            pltpu.VMEM((min(per_weight + 5, 2 * per_weight), LANES, model), bf16),
            pltpu.VMEM((2,) + wg.shape[::-1], bf16),
            pltpu.VMEM(wd.shape, bf16),
            pltpu.VMEM((n_all, rows, own), bf16),
            pltpu.VMEM((heads, rows, value_dim), f32),
            pltpu.VMEM((kv_n - 1, heads, rows, value_dim), f32),
            pltpu.VMEM((heads, rows, value_dim), f32),
            pltpu.VMEM((rows, both, value_dim), f32),
            pltpu.VMEM((rows, both, value_dim), bf16),
            pltpu.VMEM((kv_n - 1, rows, both, value_dim), bf16),
            pltpu.VMEM((rows, value_dim), f32),
            pltpu.VMEM((kv_n - 1, rows, value_dim), f32),
            pltpu.VMEM((rows, heads, value_dim), f32),
            pltpu.VMEM((rows, wo.shape[0]), bf16),
            pltpu.VMEM((n_all, rows, wo.shape[0]), bf16),
            pltpu.VMEM((rows, model), f32),
            pltpu.VMEM((rows, wg.shape[0]), bf16),
            pltpu.VMEM((n_all - 1, rows, own), bf16),
            pltpu.VMEM((n_all - 1, rows, own), bf16),
            dma((5,)), dma((2 * per_weight,)),
            dma((n_all,)), dma((n_all,)),
            dma((heads // 4, kv_n - 1)), dma((heads // 4, kv_n - 1)),
            dma((rows, kv_n - 1)), dma((rows, kv_n - 1)),
            dma((kv_n - 1,)), dma((kv_n - 1,)),
            dma((n_all - 1,)), dma((n_all - 1,)),
            dma((n_all - 1,)), dma((n_all - 1,)),
        ],
        compiler_params=pltpu.CompilerParams(
            collective_id=0, has_side_effects=True, vmem_limit_bytes=67043328
        ),
    )(
        tokens, attn_gain.reshape(1, -1), wq,
        kc.reshape(rows, positions, value_dim), vc.reshape(rows, positions, value_dim),
        lam.reshape(1, -1), hgain.reshape(1, -1), wo, mgain.reshape(1, -1), wg, wu, wd, table,
    )


def layer(kv_n, tp_n, *arrays):
    tokens, kc, wg = arrays[0], arrays[3], arrays[9]
    small = tokens.shape[0] == kv_n and kc.shape[2] == 1 and tp_n == 2
    if small and tokens.shape[1] % LANES == 0 and wg.shape[0] % LANES == 0:
        return fused(kv_n, tp_n, *arrays)
    return shards(*arrays)


def solution(mesh):
    placed = (
        P("dp", ("kv", "tp")),
        P(),
        P("kv", "tp"),
        P("dp", "kv", "tp", None),
        P("dp", "kv", "tp", None),
        P("tp"),
        P(),
        P("kv", "tp"),
        P(),
        P(("kv", "tp"), None),
        P(("kv", "tp"), None),
        P(("kv", "tp"), None),
    )
    return jax.shard_map(
        functools.partial(layer, mesh.shape["kv"], mesh.shape["tp"]),
        mesh=mesh, in_specs=placed, out_specs=P("dp", ("kv", "tp")), check_vma=False
    )
```

profile of v0, /device:TPU:0, one launch (start us, length us, event | category | flops | bytes accessed | tf_op | source)
XLA Modules:
  0.0 35.6 jit_solution(13552084557305267635)
XLA Ops:
  0.0 34.4 %shard_map.127 = bf16[4,512]{1,0:T(4,128)(2,1)} custom-call(bf16[4,512]{1,0:T(4,128)(2,1)} %tok.1, f32[1,4096]{1,0:T(1,128)} %bitcast.8, bf16[1024,2048]{1,0:T(8,128)(2,1)} %wq_h.1, bf16[4,256,128]{2,1,0:T(8,128)(2,1)} %bitcast.6, bf16[4,256,128]{2,1,0:T(8,128)(2,1)} %bitcast.7, f32[1,16]{1,0:T(1,128)} %bitcast.10, f32[1,128]{1,0:T(1,128)} %bitcast.11, ...), custom_call_target="tpu_custom_call" | custom-call | tf_op jit(solution)/shard_map/pallas_call | solution.py:472
  34.4 1.3 %copy.15 = bf16[4,512]{1,0:T(4,128)(2,1)} copy(bf16[4,512]{1,0:T(4,128)(2,1)} %shard_map.127) | data formatting | bytes 8192
where the time goes:
time: 35.9 us; the launch traced here: 35.6 us
  Pallas kernels  34.4 us (96%)
  local copies, waits for them, and re-layouts  1.28 us (4%)
    pallas_call x1, Pallas kernels, fused(): pl.pallas_call(functools.partial(same_chip_kernel, kv_n, tp_n), out_shape...  34.4 us
    unnamed x1, local copies, waits for them, and re-layouts  1.28 us

commit v1 on v0

v1 whole, which is shorter than its diff:
```python
import functools

import jax
import jax.numpy as jnp
import numpy as np
from jax import lax
from jax.experimental import pallas as pl
from jax.experimental.pallas import tpu as pltpu
from jax.sharding import PartitionSpec as P

EPS = 1e-06
THETA = 10000.0
LANES = 128
CUTS = (10, 19, 22)
AHEAD = 8


def merged(x, axis, combine):
    everything = jax.tree.map(lambda part: lax.all_gather(part, axis), x)
    first = jax.tree.map(lambda part: part[0], everything)

    def hop(k, so_far):
        return combine(so_far, jax.tree.map(lambda part: part[k], everything))

    return lax.fori_loop(1, lax.axis_size(axis), hop, first)


def rotate(vector, position):
    half_len = vector.shape[-1] // 2
    inv_freq = 1.0 / THETA ** (jnp.arange(half_len, dtype=jnp.float32) / half_len)
    angles = position * inv_freq
    cos_table = jnp.cos(angles)
    sin_table = jnp.sin(angles)
    first_half = vector[..., :half_len]
    second_half = vector[..., half_len:]
    return jnp.concatenate(
        [
            first_half * cos_table - second_half * sin_table,
            second_half * cos_table + first_half * sin_table,
        ],
        axis=-1,
    )


def combine(earlier, latter):
    peak_a, total_a, value_a = earlier
    peak_b, total_b, value_b = latter
    peak_new = jnp.maximum(peak_a, peak_b)
    factor_a = jnp.exp(peak_a - peak_new)
    factor_b = jnp.exp(peak_b - peak_new)
    return (
        peak_new,
        total_a * factor_a + total_b * factor_b,
        value_a * factor_a[..., None] + value_b * factor_b[..., None],
    )


def inner_last(left, right):
    return lax.dot_general(
        left, right, (((1,), (1,)), ((), ())), preferred_element_type=jnp.float32
    )


def shards(
    tokens,
    attn_gain,
    query_weight,
    key_cache,
    value_cache,
    head_lambda,
    head_gain,
    out_weight,
    mlp_gain,
    gate_weight,
    up_weight,
    down_weight,
):
    row_count = tokens.shape[0]
    kv_count = lax.axis_size("kv")
    tp_count = lax.axis_size("tp")
    kv_index = lax.axis_index("kv")
    row_span = query_weight.shape[0]
    full_rows = lax.all_gather(tokens, ("kv", "tp"), axis=1, tiled=True)
    wide_rows = full_rows.astype(jnp.float32)
    mean_square = jnp.mean(wide_rows * wide_rows, axis=-1, keepdims=True)
    scaled = (wide_rows * attn_gain).astype(jnp.bfloat16)
    local_cols = lax.dynamic_slice_in_dim(scaled, kv_index * row_span, row_span, 1)
    queries = lax.psum(jnp.dot(local_cols, query_weight, preferred_element_type=jnp.float32), "kv")
    queries = queries * lax.rsqrt(mean_square + EPS)
    head_count = head_lambda.shape[0]
    kv_local = key_cache.shape[2]
    group_size = head_count // kv_local
    position_count = key_cache.shape[1]
    half_dim = key_cache.shape[3] // 2
    value_dim = value_cache.shape[3]
    queries = queries.reshape(row_count, kv_local, group_size, 2, half_dim)
    rotated = rotate(queries, jnp.float32(position_count * kv_count)).astype(jnp.bfloat16)
    key_grid = key_cache.reshape(row_count, position_count, kv_local, 2, half_dim)
    scores = jnp.einsum(
        "bkgch,bpkch->bkgcp", rotated, key_grid, preferred_element_type=jnp.float32
    ) * half_dim ** (-0.5)
    local_peak = jnp.max(scores, axis=-1)
    weights_exp = jnp.exp(scores - local_peak[..., None])
    lam_grid = head_lambda.reshape(kv_local, group_size)[None, :, :, None]
    exp_total = jnp.sum(weights_exp, axis=-1)
    weighted = jnp.einsum(
        "bkgcp,bpkv->bkgcv",
        weights_exp.astype(jnp.bfloat16),
        value_cache,
        preferred_element_type=jnp.float32,
    )
    peak_all, total_all, weighted_all = merged((local_peak, exp_total, weighted), "kv", combine)
    attended = weighted_all / total_all[..., None]
    difference = attended[:, :, :, 0] - lam_grid * attended[:, :, :, 1]
    head_norm = lax.rsqrt(jnp.mean(difference * difference, axis=-1, keepdims=True) + EPS)
    head_out = (difference * head_norm * head_gain).reshape(row_count, head_count * value_dim)
    head_out = head_out.astype(jnp.bfloat16)
    out_part = inner_last(head_out, out_weight).astype(jnp.bfloat16)
    pieces = lax.all_gather(out_part, ("kv", "tp"), axis=1, tiled=True)
    attention = jnp.sum(
        pieces.astype(jnp.float32).reshape(row_count, kv_count, tp_count, -1), axis=2
    )
    stream = wide_rows + attention.reshape(row_count, -1)
    stream_square = jnp.mean(stream * stream, axis=-1, keepdims=True)
    normed = (stream * lax.rsqrt(stream_square + EPS) * mlp_gain).astype(jnp.bfloat16)
    gate_out = inner_last(normed, gate_weight)
    up_out = inner_last(normed, up_weight)
    hidden = (jax.nn.silu(gate_out) * up_out).astype(jnp.bfloat16)
    own_cols = tokens.shape[1]
    down_cols = lax.psum_scatter(
        lax.dot_general(
            down_weight, hidden, (((0,), (1,)), ((), ())), preferred_element_type=jnp.float32
        ),
        ("kv", "tp"),
        scatter_dimension=0,
        tiled=True,
    )
    column_index = lax.axis_index(("kv", "tp"))
    own_stream = lax.dynamic_slice_in_dim(stream, column_index * own_cols, own_cols, 1)
    return (own_stream + down_cols.T).astype(jnp.bfloat16)


def fused_kernel(
    kv_n, tp_n, tok_h, again_h, wq_h, kc_h, vc_h, lam_h, hgain_h, wo_h, mgain_h, wg_h, wu_h, wd_h,
    table_h,
    out,
    again, lam, hgain, mgain, table,
    wq, kc, vc, wo, stage, wgu_t, wd,
    tg, qa, qf, ms, mb, mv, st, cf, hf, og, stream, ga, hid, ds, dr,
    hand, lsem, wqsem, wsem, csem,
    tsend, trecv, qsend, qrecv, ssend, srecv, msend, mrecv, osend, orecv, dsend, drecv,
):
    kv, tp = lax.axis_index("kv"), lax.axis_index("tp")
    n_all = kv_n * tp_n
    me = kv * tp_n + tp
    rows, own = tg.shape[1:]
    mate = {"kv": kv, "tp": lax.rem(tp + 1, tp_n)}
    heads, value_dim = hf.shape[1], hf.shape[2]
    both = 2 * heads
    features = wo.shape[0]
    units = wd.shape[0]
    per_weight = units // LANES
    chunks = 2 * per_weight
    slots = stage.shape[0]
    per = 4
    pieces = heads // per
    width = per * value_dim

    def query_load(j):
        cols = pl.ds(j * width, width)
        return pltpu.make_async_copy(wq_h.at[:, cols], wq.at[:, cols], wqsem.at[j])

    token_load = pltpu.make_async_copy(tok_h, tg.at[me], lsem.at[0])
    token_load.start()
    for j in range(pieces):
        query_load(j).start()
    small_loads = [
        pltpu.make_async_copy(source, target, lsem.at[slot + 1])
        for slot, (source, target) in enumerate(
            [(again_h, again), (table_h, table), (lam_h, lam), (hgain_h, hgain), (mgain_h, mgain)]
        )
    ]
    for load in small_loads:
        load.start()

    def chunk_load(weight, i, slot):
        piece = pl.ds(pl.multiple_of(i * LANES, LANES), LANES)
        at = i if weight is wg_h else i + per_weight
        return pltpu.make_async_copy(weight.at[piece], stage.at[slot], csem.at[at])

    def later_load(i):
        @pl.when(i < per_weight)
        def _():
            chunk_load(wg_h, i, lax.rem(i, slots)).start()

        @pl.when((i >= per_weight) & (i < chunks))
        def _():
            chunk_load(wu_h, i - per_weight, lax.rem(i, slots)).start()

    def turn(low, high):
        def turn_gate(i, carry):
            slot = lax.rem(i, slots)
            later_load(i + AHEAD)
            chunk_load(wg_h, i, slot).wait()
            at = pl.ds(pl.multiple_of(i * LANES, LANES), LANES)
            wgu_t[0, :, at] = stage[slot].T
            return carry

        def turn_up(i, carry):
            slot = lax.rem(i + per_weight, slots)
            later_load(i + per_weight + AHEAD)
            chunk_load(wu_h, i, slot).wait()
            at = pl.ds(pl.multiple_of(i * LANES, LANES), LANES)
            wgu_t[1, :, at] = stage[slot].T
            return carry

        low, high = chunks * low // 22, chunks * high // 22
        if low < per_weight:
            lax.fori_loop(low, min(high, per_weight), turn_gate, 0)
        if high > per_weight:
            lax.fori_loop(max(low, per_weight) - per_weight, high - per_weight, turn_up, 0)

    half_way = kv_n // 2

    def far(i):
        down = kv_n - 1 - i
        down = down - 1 + lax.div(down - kv + kv_n - 1, kv_n)
        up = i + 1 - lax.div(kv - i + kv_n - 1, kv_n)
        low = 1 - lax.div(kv, half_way)
        return up + low * (down - up)

    others = [far(i) for i in range(kv_n - 1)]

    def remote(src, dst, send, recv, where):
        copy = pltpu.make_async_remote_copy(
            src_ref=src, dst_ref=dst, send_sem=send, recv_sem=recv,
            device_id=where, device_id_type=pl.DeviceIdType.MESH,
        )
        copy.start()
        return copy

    def arrived(dst, recv):
        pltpu.make_async_remote_copy(
            src_ref=dst, dst_ref=dst, send_sem=recv, recv_sem=recv,
            device_id=mate, device_id_type=pl.DeviceIdType.MESH,
        ).wait_recv()

    def signal(semaphore, where):
        pl.semaphore_signal(
            semaphore, inc=1, device_id=where, device_id_type=pl.DeviceIdType.MESH
        )

    barrier = pltpu.get_barrier_semaphore()
    for z in others:
        signal(barrier, {"kv": z, "tp": tp_n - 1})

    @pl.when(tp == tp_n - 1)
    def _():
        signal(barrier, mate)

    @pl.when(tp == 0)
    def _():
        pl.semaphore_wait(barrier, 1)
        signal(hand.at[0], mate)

    @pl.when(tp == tp_n - 1)
    def _():
        pl.semaphore_wait(hand.at[0], 1)

    sends = []
    token_load.wait()
    sends.append(remote(tg.at[me], tg.at[me], tsend.at[0], trecv.at[me], mate))
    small_loads[0].wait()
    at_mate = kv * tp_n + lax.rem(tp + 1, tp_n)
    arrived(tg.at[at_mate], trecv.at[at_mate])
    parts = []
    square = jnp.zeros((rows, 1), jnp.float32)
    for side in range(tp_n):
        at = kv * tp_n + side
        gain = again[:, pl.ds(pl.multiple_of(at * own, LANES), own)]
        wide = tg[at].astype(jnp.float32)
        square = square + jnp.sum(wide * wide, axis=1, keepdims=True)
        parts.append((wide * gain).astype(jnp.bfloat16))
    scaled = jnp.concatenate(parts, axis=1)
    qa[kv, heads] = jnp.broadcast_to(square, (rows, value_dim))

    def query_piece(j):
        query_load(j).wait()
        product = jnp.dot(
            scaled, wq[:, j * width:(j + 1) * width], preferred_element_type=jnp.float32
        )
        for i in range(per):
            qa[kv, j * per + i] = product[:, i * value_dim:(i + 1) * value_dim]

    def query_part(j):
        return pl.ds(j * per, per + (1 if j == pieces - 1 else 0))

    key_load = pltpu.make_async_copy(kc_h, kc, wsem.at[0])
    value_load = pltpu.make_async_copy(vc_h, vc, wsem.at[1])
    out_load = pltpu.make_async_copy(wo_h, wo, wsem.at[2])
    down_load = pltpu.make_async_copy(wd_h, wd, wsem.at[3])

    for j in range(pieces):
        query_piece(j)
        if j == 0:
            key_load.start()
            value_load.start()
            for i in range(AHEAD):
                if i < per_weight:
                    chunk_load(wg_h, i, i % slots).start()
                elif i < chunks:
                    chunk_load(wu_h, i - per_weight, i % slots).start()

            @pl.when(tp == tp_n - 1)
            def _():
                pl.semaphore_wait(barrier, tp_n * (kv_n - 1))
                signal(hand.at[1], mate)

            @pl.when(tp == 0)
            def _():
                pl.semaphore_wait(hand.at[1], 1)

        part = query_part(j)
        for i, z in enumerate(others):
            sends.append(
                remote(
                    qa.at[kv, part], qa.at[kv, part],
                    qsend.at[j, i], qrecv.at[j, kv], {"kv": z, "tp": tp},
                )
            )

    slot = 1
    for z in others:
        for side in range(tp_n):
            sends.append(
                remote(
                    tg.at[me], tg.at[me], tsend.at[slot], trecv.at[me], {"kv": z, "tp": side}
                )
            )
            slot += 1

    turn(0, CUTS[0])
    out_load.start()
    for load in small_loads[1:]:
        load.wait()
    for z in others[::-1]:
        for j in range(pieces):
            arrived(qa.at[z, query_part(j)], qrecv.at[j, z])
    square = qa[0, heads]
    for z in range(1, kv_n):
        square = square + qa[z, heads]
    scale = lax.rsqrt(square / (n_all * own) + EPS)
    lane = lax.broadcasted_iota(jnp.int32, (rows, value_dim), 1)
    half = value_dim // 2
    first = lax.rem(lane, half) < half // 2
    cosines = table[0:1, :]
    sines = table[1:2, :]
    for h in range(heads):
        total = qa[0, h]
        for z in range(1, kv_n):
            total = total + qa[z, h]
        total = total * scale
        swapped = jnp.where(
            first,
            pltpu.roll(total, value_dim - half // 2, 1),
            pltpu.roll(total, half // 2, 1),
        )
        qf[h] = total * cosines + swapped * sines

    key_load.wait()
    value_load.wait()
    low = lax.broadcasted_iota(jnp.int32, (heads, value_dim), 1) < half
    row_at = lax.broadcasted_iota(jnp.int32, (both, value_dim), 0)
    lane_at = lax.broadcasted_iota(jnp.int32, (both, value_dim), 1)
    spread = []
    for b in range(rows):
        query = qf[:, b, :]
        grid = jnp.concatenate(
            [jnp.where(low, query, 0.0), jnp.where(low, 0.0, query)], axis=0
        ).astype(jnp.bfloat16)
        scores = inner_last(grid, kc[b]) * half ** (-0.5)
        peak = jnp.max(scores, axis=1, keepdims=True)
        exps = jnp.exp(scores - peak)
        sums = jnp.sum(exps, axis=1, keepdims=True)
        spread.append(exps.astype(jnp.bfloat16))
        stats = jnp.where(lane_at == row_at, peak, 0.0) + jnp.where(
            lane_at == row_at + both, sums, 0.0
        )
        st[kv, b:b + 1, :] = jnp.sum(stats, axis=0, keepdims=True)
    for i, z in enumerate(others):
        sends.append(
            remote(
                st.at[kv], st.at[kv], ssend.at[i], srecv.at[kv], {"kv": z, "tp": tp}
            )
        )
    for b in range(rows):
        values = jnp.dot(spread[b], vc[b], preferred_element_type=jnp.float32)
        ms[b] = values
        mb[b] = values.astype(jnp.bfloat16)
    for b in range(rows):
        for i, z in enumerate(others):
            sends.append(
                remote(
                    mb.at[b], mv.at[kv, b],
                    msend.at[b, i], mrecv.at[b, kv], {"kv": z, "tp": tp},
                )
            )

    down_load.start()
    turn(CUTS[0], CUTS[1])
    lam_at = lax.broadcasted_iota(jnp.int32, (heads, heads), 0)
    lam_lane = lax.broadcasted_iota(jnp.int32, (heads, heads), 1)
    lam_col = jnp.sum(
        jnp.where(lam_at == lam_lane, lam[...], 0.0), axis=1, keepdims=True
    )
    signs = jnp.concatenate([jnp.ones((heads, 1), jnp.float32), -lam_col], axis=0)
    sources = [kv] + others[::-1]
    for z in sources[1:]:
        arrived(st.at[z], srecv.at[z])
    for b in range(rows):
        peaks, sums = [], []
        for z in sources:
            stats = st[z, b:b + 1, :]
            peaks.append(
                jnp.sum(jnp.where(lane_at == row_at, stats, 0.0), axis=1, keepdims=True)
            )
            sums.append(
                jnp.sum(jnp.where(lane_at == row_at + both, stats, 0.0), axis=1, keepdims=True)
            )
        top = peaks[0]
        for peak in peaks[1:]:
            top = jnp.maximum(top, peak)
        factors = [jnp.exp(peak - top) for peak in peaks]
        all_sums = jnp.zeros_like(top)
        for factor, total in zip(factors, sums):
            all_sums = all_sums + total * factor
        share = signs / all_sums
        for at, factor in enumerate(factors):
            cf[at, b] = jnp.broadcast_to(factor * share, (both, value_dim))
    for b in range(rows):
        for z in sources[1:]:
            arrived(mv.at[z, b], mrecv.at[b, z])
    for b in range(rows):
        weighted = ms[b] * cf[0, b]
        for at, z in enumerate(sources[1:]):
            weighted = weighted + mv[z, b].astype(jnp.float32) * cf[at + 1, b]
        difference = weighted[0:heads] + weighted[heads:both]
        norm = lax.rsqrt(jnp.mean(difference * difference, axis=1, keepdims=True) + EPS)
        hf[b] = difference * norm * hgain[...]
    flat = jnp.concatenate(
        [hf[:, h, :] for h in range(heads)], axis=1
    ).astype(jnp.bfloat16)
    out_load.wait()
    cut = features // 2
    for j in range(2):
        cols = pl.ds(j * cut, cut)
        og[me, :, cols] = inner_last(flat, wo[j * cut:(j + 1) * cut, :]).astype(jnp.bfloat16)
        slot = 0
        for z in others:
            for side in range(tp_n):
                sends.append(
                    remote(
                        og.at[me, :, cols], og.at[me, :, cols],
                        osend.at[j, slot], orecv.at[j, me], {"kv": z, "tp": side},
                    )
                )
                slot += 1
        sends.append(
            remote(
                og.at[me, :, cols], og.at[me, :, cols], osend.at[j, slot], orecv.at[j, me], mate
            )
        )

    turn(CUTS[1], CUTS[2])
    for z in others:
        for side in range(tp_n):
            at = z * tp_n + side
            arrived(tg.at[at], trecv.at[at])
    square = jnp.zeros((rows, 1), jnp.float32)
    for order, z in enumerate(sources):
        for side in range(tp_n):
            at = z * tp_n + side
            for j in range(2):
                cols = pl.ds(j * cut, cut)
                if order == 0:
                    continue
                arrived(og.at[at, :, cols], orecv.at[j, at])
        if order == 0:
            for j in range(2):
                cols = pl.ds(j * cut, cut)
                arrived(og.at[at_mate, :, cols], orecv.at[j, at_mate])
        tokens = jnp.concatenate(
            [tg[z * tp_n + side].astype(jnp.float32) for side in range(tp_n)], axis=1
        )
        attention = og[z * tp_n].astype(jnp.float32)
        for side in range(1, tp_n):
            attention = attention + og[z * tp_n + side].astype(jnp.float32)
        piece = tokens + attention
        at = pl.ds(pl.multiple_of(z * features, LANES), features)
        stream[:, at] = piece
        square = square + jnp.sum(piece * piece, axis=1, keepdims=True)
        gained = (piece * mgain[:, at]).astype(jnp.bfloat16)
        for g in range(2):
            product = jnp.dot(gained, wgu_t[g, at, :], preferred_element_type=jnp.float32)
            if order == 0:
                ga[g] = product
            else:
                ga[g] = ga[g] + product
    scale = lax.rsqrt(square / (n_all * own) + EPS)
    gate = ga[0] * scale
    up = ga[1] * scale
    hid[...] = (gate / (1.0 + jnp.exp(-gate)) * up).astype(jnp.bfloat16)
    hidden = hid[...]
    down_load.wait()

    def down_block(at):
        return jnp.dot(
            hidden,
            wd[:, pl.ds(pl.multiple_of(at * own, LANES), own)],
            preferred_element_type=jnp.float32,
        )

    targets = []
    for z in others:
        for side in range(tp_n):
            targets.append((z * tp_n + side, {"kv": z, "tp": side}))
    targets.append((at_mate, mate))
    pending = None

    def down_send(slot, block):
        at, where = targets[slot]
        ds[at] = block.astype(ds.dtype)
        sends.append(
            remote(ds.at[at], dr.at[me], dsend.at[slot], drecv.at[me], where)
        )

    for slot, (at, _) in enumerate(targets):
        block = down_block(at)
        if pending is not None:
            down_send(slot - 1, pending)
        pending = block
    total = down_block(me)
    down_send(len(targets) - 1, pending)
    total = total + stream[:, pl.ds(pl.multiple_of(me * own, LANES), own)]
    arrived(dr.at[at_mate], drecv.at[at_mate])
    total = total + dr[at_mate].astype(jnp.float32)
    for z in others[::-1]:
        for side in range(tp_n):
            at = z * tp_n + side
            arrived(dr.at[at], drecv.at[at])
    for z in others[::-1]:
        for side in range(tp_n):
            total = total + dr[z * tp_n + side].astype(jnp.float32)
    out[...] = total.astype(out.dtype)
    for copy in sends:
        copy.wait_send()


def turning(head_dim, position):
    half_len = head_dim // 4
    inv_freq = np.float32(1.0) / np.float32(THETA) ** (
        np.arange(half_len, dtype=np.float32) / np.float32(half_len)
    )
    angles = (np.float32(position) * inv_freq.astype(np.float32)).astype(np.float32)
    cos, sin = np.cos(angles), np.sin(angles)
    return np.stack(
        [np.concatenate([cos, cos] * 2), np.concatenate([-sin, sin] * 2)]
    ).astype(np.float32)


def fused(kv_n, tp_n, *arrays):
    (tokens, attn_gain, wq, kc, vc, lam, hgain, wo, mgain, wg, wu, wd) = arrays
    rows, own = tokens.shape
    n_all = kv_n * tp_n
    positions, value_dim = kc.shape[1], kc.shape[3]
    heads = lam.shape[0]
    both = 2 * heads
    model = n_all * own
    per_weight = wg.shape[0] // LANES
    pieces = heads // 4
    f32, bf16 = jnp.float32, jnp.bfloat16
    table = jnp.asarray(turning(value_dim, positions * kv_n))
    dma = pltpu.SemaphoreType.DMA
    hbm = pl.BlockSpec(memory_space=pl.ANY)
    return pl.pallas_call(
        functools.partial(fused_kernel, kv_n, tp_n),
        out_shape=pltpu.VMEM((rows, own), tokens.dtype),
        in_specs=[hbm] * 13,
        out_specs=pl.BlockSpec(memory_space=pltpu.VMEM),
        scratch_shapes=[
            pltpu.VMEM((1, model), f32),
            pltpu.VMEM((1, heads), f32),
            pltpu.VMEM((1, value_dim), f32),
            pltpu.VMEM((1, model), f32),
            pltpu.VMEM((2, value_dim), f32),
            pltpu.VMEM(wq.shape, bf16),
            pltpu.VMEM((rows, positions, value_dim), bf16),
            pltpu.VMEM((rows, positions, value_dim), bf16),
            pltpu.VMEM(wo.shape, bf16),
            pltpu.VMEM((min(AHEAD + 1, 2 * per_weight), LANES, model), bf16),
            pltpu.VMEM((2,) + wg.shape[::-1], bf16),
            pltpu.VMEM(wd.shape, bf16),
            pltpu.VMEM((n_all, rows, own), bf16),
            pltpu.VMEM((kv_n, heads + 1, rows, value_dim), f32),
            pltpu.VMEM((heads, rows, value_dim), f32),
            pltpu.VMEM((rows, both, value_dim), f32),
            pltpu.VMEM((rows, both, value_dim), bf16),
            pltpu.VMEM((kv_n, rows, both, value_dim), bf16),
            pltpu.VMEM((kv_n, rows, value_dim), f32),
            pltpu.VMEM((kv_n, rows, both, value_dim), f32),
            pltpu.VMEM((rows, heads, value_dim), f32),
            pltpu.VMEM((n_all, rows, wo.shape[0]), bf16),
            pltpu.VMEM((rows, model), f32),
            pltpu.VMEM((2, rows, wg.shape[0]), f32),
            pltpu.VMEM((rows, wg.shape[0]), bf16),
            pltpu.VMEM((n_all, rows, own), bf16),
            pltpu.VMEM((n_all, rows, own), bf16),
            pltpu.SemaphoreType.REGULAR((2,)),
            dma((6,)), dma((pieces,)), dma((4,)), dma((2 * per_weight,)),
            dma((n_all,)), dma((n_all,)),
            dma((pieces, kv_n - 1)), dma((pieces, kv_n)),
            dma((kv_n - 1,)), dma((kv_n,)),
            dma((rows, kv_n - 1)), dma((rows, kv_n)),
            dma((2, n_all - 1)), dma((2, n_all)),
            dma((n_all - 1,)), dma((n_all,)),
        ],
        compiler_params=pltpu.CompilerParams(
            collective_id=0, has_side_effects=True, vmem_limit_bytes=65000000
        ),
    )(
        tokens, attn_gain.reshape(1, -1), wq,
        kc.reshape(rows, positions, value_dim), vc.reshape(rows, positions, value_dim),
        lam.reshape(1, -1), hgain.reshape(1, -1), wo, mgain.reshape(1, -1), wg, wu, wd, table,
    )


def layer(kv_n, tp_n, *arrays):
    tokens, kc, wg = arrays[0], arrays[3], arrays[9]
    small = tokens.shape[0] == kv_n and kc.shape[2] == 1 and tp_n == 2
    if small and tokens.shape[1] % LANES == 0 and wg.shape[0] % LANES == 0:
        return fused(kv_n, tp_n, *arrays)
    return shards(*arrays)


def solution(mesh):
    placed = (
        P("dp", ("kv", "tp")),
        P(),
        P("kv", "tp"),
        P("dp", "kv", "tp", None),
        P("dp", "kv", "tp", None),
        P("tp"),
        P(),
        P("kv", "tp"),
        P(),
        P(("kv", "tp"), None),
        P(("kv", "tp"), None),
        P(("kv", "tp"), None),
    )
    return jax.shard_map(
        functools.partial(layer, mesh.shape["kv"], mesh.shape["tp"]),
        mesh=mesh, in_specs=placed, out_specs=P("dp", ("kv", "tp")), check_vma=False
    )
```

time: 35.9 us -> 28.3 us (0.79)
  Pallas kernels: 34.4 us -> 27.5 us
  local copies, waits for them, and re-layouts: 1.28 us -> 0.6 us
    pallas_call x1, Pallas kernels: 34.4 us -> 27.5 us  [fused(): pl.pallas_call(functools.partial(fused_kernel, kv_n, tp_n), out_shape=plt...]
    unnamed x1, local copies, waits for them, and re-layouts: 1.28 us -> 0.6 us
where the time goes in v1:
time: 28.3 us; the launch traced here: 28.1 us
  Pallas kernels  27.5 us (97%)
  local copies, waits for them, and re-layouts  0.6 us (2%)
    pallas_call x1, Pallas kernels, fused(): pl.pallas_call(functools.partial(fused_kernel, kv_n, tp_n), out_shape=plt...  27.5 us
    unnamed x1, local copies, waits for them, and re-layouts  0.6 us

profile of v1, /device:TPU:0, one launch (start us, length us, event | category | flops | bytes accessed | tf_op | source)
XLA Modules:
  0.0 28.1 jit_solution(5523955028197348130)
XLA Ops:
  0.0 27.5 %shard_map.127 = bf16[4,512]{1,0:T(4,128)(2,1)S(1)} custom-call(bf16[4,512]{1,0:T(4,128)(2,1)} %tok_h.1, f32[1,4096]{1,0:T(1,128)} %bitcast.8, bf16[1024,2048]{1,0:T(8,128)(2,1)} %wq_h.1, bf16[4,256,128]{2,1,0:T(8,128)(2,1)} %bitcast.6, bf16[4,256,128]{2,1,0:T(8,128)(2,1)} %bitcast.7, f32[1,16]{1,0:T(1,128)} %bitcast.10, f32[1,128]{1,0:T(1,128)} %bitcast.11, ...), custom_call_target="tpu_custom_call" | custom-call | tf_op jit(solution)/shard_map/pallas_call | solution.py:585
  27.5 0.6 %copy.15 = bf16[4,512]{1,0:T(4,128)(2,1)} copy(bf16[4,512]{1,0:T(4,128)(2,1)S(1)} %shard_map.127) | data formatting | bytes 8192

commit v2 on v1

v2 whole, which is shorter than its diff:
```python
import functools

import jax
import jax.numpy as jnp
import numpy as np
from jax import lax
from jax.experimental import pallas as pl
from jax.experimental.pallas import tpu as pltpu
from jax.sharding import PartitionSpec as P

EPS = 1e-06
THETA = 10000.0
LANES = 128
AHEAD = 8
MARKS = (0, 4, 8, 9, 10, 14, 15, 17, 22)


def merged(x, axis, combine):
    everything = jax.tree.map(lambda part: lax.all_gather(part, axis), x)
    first = jax.tree.map(lambda part: part[0], everything)

    def hop(k, so_far):
        return combine(so_far, jax.tree.map(lambda part: part[k], everything))

    return lax.fori_loop(1, lax.axis_size(axis), hop, first)


def rotate(vector, position):
    half_len = vector.shape[-1] // 2
    inv_freq = 1.0 / THETA ** (jnp.arange(half_len, dtype=jnp.float32) / half_len)
    angles = position * inv_freq
    cos_table = jnp.cos(angles)
    sin_table = jnp.sin(angles)
    first_half = vector[..., :half_len]
    second_half = vector[..., half_len:]
    return jnp.concatenate(
        [
            first_half * cos_table - second_half * sin_table,
            second_half * cos_table + first_half * sin_table,
        ],
        axis=-1,
    )


def combine(earlier, latter):
    peak_a, total_a, value_a = earlier
    peak_b, total_b, value_b = latter
    peak_new = jnp.maximum(peak_a, peak_b)
    factor_a = jnp.exp(peak_a - peak_new)
    factor_b = jnp.exp(peak_b - peak_new)
    return (
        peak_new,
        total_a * factor_a + total_b * factor_b,
        value_a * factor_a[..., None] + value_b * factor_b[..., None],
    )


def inner_last(left, right):
    return lax.dot_general(
        left, right, (((1,), (1,)), ((), ())), preferred_element_type=jnp.float32
    )


def shards(
    tokens,
    attn_gain,
    query_weight,
    key_cache,
    value_cache,
    head_lambda,
    head_gain,
    out_weight,
    mlp_gain,
    gate_weight,
    up_weight,
    down_weight,
):
    row_count = tokens.shape[0]
    kv_count = lax.axis_size("kv")
    tp_count = lax.axis_size("tp")
    kv_index = lax.axis_index("kv")
    row_span = query_weight.shape[0]
    full_rows = lax.all_gather(tokens, ("kv", "tp"), axis=1, tiled=True)
    wide_rows = full_rows.astype(jnp.float32)
    mean_square = jnp.mean(wide_rows * wide_rows, axis=-1, keepdims=True)
    scaled = (wide_rows * attn_gain).astype(jnp.bfloat16)
    local_cols = lax.dynamic_slice_in_dim(scaled, kv_index * row_span, row_span, 1)
    queries = lax.psum(jnp.dot(local_cols, query_weight, preferred_element_type=jnp.float32), "kv")
    queries = queries * lax.rsqrt(mean_square + EPS)
    head_count = head_lambda.shape[0]
    kv_local = key_cache.shape[2]
    group_size = head_count // kv_local
    position_count = key_cache.shape[1]
    half_dim = key_cache.shape[3] // 2
    value_dim = value_cache.shape[3]
    queries = queries.reshape(row_count, kv_local, group_size, 2, half_dim)
    rotated = rotate(queries, jnp.float32(position_count * kv_count)).astype(jnp.bfloat16)
    key_grid = key_cache.reshape(row_count, position_count, kv_local, 2, half_dim)
    scores = jnp.einsum(
        "bkgch,bpkch->bkgcp", rotated, key_grid, preferred_element_type=jnp.float32
    ) * half_dim ** (-0.5)
    local_peak = jnp.max(scores, axis=-1)
    weights_exp = jnp.exp(scores - local_peak[..., None])
    lam_grid = head_lambda.reshape(kv_local, group_size)[None, :, :, None]
    exp_total = jnp.sum(weights_exp, axis=-1)
    weighted = jnp.einsum(
        "bkgcp,bpkv->bkgcv",
        weights_exp.astype(jnp.bfloat16),
        value_cache,
        preferred_element_type=jnp.float32,
    )
    peak_all, total_all, weighted_all = merged((local_peak, exp_total, weighted), "kv", combine)
    attended = weighted_all / total_all[..., None]
    difference = attended[:, :, :, 0] - lam_grid * attended[:, :, :, 1]
    head_norm = lax.rsqrt(jnp.mean(difference * difference, axis=-1, keepdims=True) + EPS)
    head_out = (difference * head_norm * head_gain).reshape(row_count, head_count * value_dim)
    head_out = head_out.astype(jnp.bfloat16)
    out_part = inner_last(head_out, out_weight).astype(jnp.bfloat16)
    pieces = lax.all_gather(out_part, ("kv", "tp"), axis=1, tiled=True)
    attention = jnp.sum(
        pieces.astype(jnp.float32).reshape(row_count, kv_count, tp_count, -1), axis=2
    )
    stream = wide_rows + attention.reshape(row_count, -1)
    stream_square = jnp.mean(stream * stream, axis=-1, keepdims=True)
    normed = (stream * lax.rsqrt(stream_square + EPS) * mlp_gain).astype(jnp.bfloat16)
    gate_out = inner_last(normed, gate_weight)
    up_out = inner_last(normed, up_weight)
    hidden = (jax.nn.silu(gate_out) * up_out).astype(jnp.bfloat16)
    own_cols = tokens.shape[1]
    down_cols = lax.psum_scatter(
        lax.dot_general(
            down_weight, hidden, (((0,), (1,)), ((), ())), preferred_element_type=jnp.float32
        ),
        ("kv", "tp"),
        scatter_dimension=0,
        tiled=True,
    )
    column_index = lax.axis_index(("kv", "tp"))
    own_stream = lax.dynamic_slice_in_dim(stream, column_index * own_cols, own_cols, 1)
    return (own_stream + down_cols.T).astype(jnp.bfloat16)


def fused_kernel(
    kv_n, tp_n, tok_h, again_h, wq_h, kc_h, vc_h, lam_h, hgain_h, wo_h, mgain_h, wg_h, wu_h, wd_h,
    table_h,
    out,
    again, lam, hgain, mgain, table,
    wq, kc, vc, wo, wo_t, stage, wgu_t, wd,
    tg, qa, qf, ms, mv, st, cf, hf, oa, og, stream, ga, hid, ds, dr,
    hand, lsem, wsem, csem, sent, trecv, qrecv, srecv, mrecv, orecv, drecv,
):
    kv, tp = lax.axis_index("kv"), lax.axis_index("tp")
    n_all = kv_n * tp_n
    me = kv * tp_n + tp
    rows, own = tg.shape[1:]
    mate = {"kv": kv, "tp": lax.rem(tp + 1, tp_n)}
    heads, value_dim = qf.shape[0], qf.shape[2]
    group = heads // 2
    both = 2 * group
    features = wo.shape[0]
    units = wd.shape[0]
    per_weight = units // LANES
    chunks = 2 * per_weight
    slots = stage.shape[0]

    span = group * value_dim

    def query_load(side, g):
        at = pl.ds(pl.multiple_of(lax.rem(tp + side, tp_n) * own, LANES), own)
        cols = pl.ds(g * span, span)
        return pltpu.make_async_copy(
            wq_h.at[at, cols], wq.at[at, cols], wsem.at[side * 2 + g]
        )

    token_load = pltpu.make_async_copy(tok_h, tg.at[me], lsem.at[0])
    token_load.start()
    for side in range(2):
        for g in range(2):
            query_load(side, g).start()
    small_loads = [
        pltpu.make_async_copy(source, target, lsem.at[slot + 1])
        for slot, (source, target) in enumerate(
            [(again_h, again), (table_h, table), (lam_h, lam), (hgain_h, hgain), (mgain_h, mgain)]
        )
    ]
    for load in small_loads:
        load.start()

    down_rows = units // AHEAD
    marks = [chunks * mark // MARKS[-1] for mark in MARKS]

    def chunk_load(weight, i, slot):
        piece = pl.ds(pl.multiple_of(i * LANES, LANES), LANES)
        return pltpu.make_async_copy(weight.at[piece], stage.at[slot], csem.at[slot])

    def down_piece(i):
        piece = pl.ds(pl.multiple_of(i * down_rows, 8), down_rows)
        return pltpu.make_async_copy(wd_h.at[piece], wd.at[piece], wsem.at[3])

    def start_load(i):
        if isinstance(i, int):
            if i < per_weight:
                chunk_load(wg_h, i, i % slots).start()
            elif i < chunks:
                chunk_load(wu_h, i - per_weight, i % slots).start()
            else:
                down_piece(i - chunks).start()
            return

        @pl.when(i < per_weight)
        def _():
            chunk_load(wg_h, i, lax.rem(i, slots)).start()

        @pl.when((i >= per_weight) & (i < chunks))
        def _():
            chunk_load(wu_h, i - per_weight, lax.rem(i, slots)).start()

        @pl.when(i >= chunks)
        def _():
            down_piece(i - chunks).start()

    def loaded(which):
        for i in which:
            start_load(i + AHEAD)
        for i in which:
            slot = i % slots if isinstance(i, int) else lax.rem(i, slots)
            chunk_load(wg_h, 0, slot).wait()

    def transpose(which):
        for i in which:
            if isinstance(i, int):
                slot, weight, at = i % slots, i // per_weight, i % per_weight * LANES
            else:
                slot, weight = lax.rem(i, slots), lax.div(i, per_weight)
                at = pl.multiple_of(lax.rem(i, per_weight) * LANES, LANES)
            wgu_t[weight, :, pl.ds(at, LANES)] = stage[slot].T

    def turn(low, high):
        def pair(i, carry):
            which = (low + 2 * i, low + 2 * i + 1)
            loaded(which)
            transpose(which)
            return carry

        lax.fori_loop(0, (high - low) // 2, pair, 0)
        if (high - low) % 2:
            loaded((high - 1,))
            transpose((high - 1,))

    def turn_out():
        def pair(i, carry):
            for side in range(2):
                at = pl.ds(pl.multiple_of((2 * i + side) * LANES, LANES), LANES)
                wo_t[:, at] = wo[at, :].T
            return carry

        lax.fori_loop(0, features // LANES // 2, pair, 0)

    half_way = kv_n // 2

    def far(i):
        down = kv_n - 1 - i
        down = down - 1 + lax.div(down - kv + kv_n - 1, kv_n)
        up = i + 1 - lax.div(kv - i + kv_n - 1, kv_n)
        low = 1 - lax.div(kv, half_way)
        return up + low * (down - up)

    others = [far(i) for i in range(kv_n - 1)]

    def remote(ref, send, recv, where, target=None):
        pltpu.make_async_remote_copy(
            src_ref=ref, dst_ref=ref if target is None else target, send_sem=sent.at[send],
            recv_sem=recv, device_id=where, device_id_type=pl.DeviceIdType.MESH,
        ).start()

    def batch(ref, send, recv):
        return pltpu.make_async_remote_copy(
            src_ref=ref, dst_ref=ref, send_sem=send, recv_sem=recv,
            device_id=mate, device_id_type=pl.DeviceIdType.MESH,
        )

    def arrived(ref, recv):
        batch(ref, recv, recv).wait_recv()

    def signal(semaphore, where):
        pl.semaphore_signal(
            semaphore, inc=1, device_id=where, device_id_type=pl.DeviceIdType.MESH
        )

    barrier = pltpu.get_barrier_semaphore()
    for z in others:
        signal(barrier, {"kv": z, "tp": tp_n - 1})

    @pl.when(tp == tp_n - 1)
    def _():
        signal(barrier, mate)

    @pl.when(tp == 0)
    def _():
        pl.semaphore_wait(barrier, 1)
        signal(hand.at[0], mate)

    @pl.when(tp == tp_n - 1)
    def _():
        pl.semaphore_wait(hand.at[0], 1)

    token_load.wait()
    remote(tg.at[me], 0, trecv.at[0], mate)
    small_loads[0].wait()
    at_mate = kv * tp_n + lax.rem(tp + 1, tp_n)
    def scaled_half(side):
        at = kv * tp_n + lax.rem(tp + side, tp_n)
        gain = again[:, pl.ds(pl.multiple_of(at * own, LANES), own)]
        wide = tg[at].astype(jnp.float32)
        return (wide * gain).astype(jnp.bfloat16), jnp.sum(wide * wide, axis=1, keepdims=True)

    def half_product(scaled, side, g):
        query_load(side, g).wait()
        at = pl.ds(pl.multiple_of(lax.rem(tp + side, tp_n) * own, LANES), own)
        return jnp.dot(
            scaled, wq[at, g * span:(g + 1) * span], preferred_element_type=jnp.float32
        )

    def query_group(g):
        return pl.ds(g * (group + 1), group + 1 - g)

    scaled, own_square = scaled_half(0)
    partial = [half_product(scaled, 0, g) for g in range(2)]
    key_load = pltpu.make_async_copy(kc_h, kc, wsem.at[0])
    value_load = pltpu.make_async_copy(vc_h, vc, wsem.at[1])
    out_load = pltpu.make_async_copy(wo_h, wo, wsem.at[2])
    down_load = pltpu.make_async_copy(wd_h, wd, wsem.at[3])
    key_load.start()
    value_load.start()
    for i in range(AHEAD):
        start_load(i)
    arrived(tg.at[at_mate], trecv.at[0])
    scaled, square = scaled_half(1)
    qa[kv, 0] = jnp.broadcast_to(own_square + square, (rows, value_dim))


    def query_half(g):
        product = partial[g] + half_product(scaled, 1, g)
        for i in range(group):
            qa[kv, 1 + g * group + i] = product[:, i * value_dim:(i + 1) * value_dim]

    query_half(0)
    @pl.when(tp == tp_n - 1)
    def _():
        pl.semaphore_wait(barrier, tp_n * (kv_n - 1))
        signal(hand.at[1], mate)

    @pl.when(tp == 0)
    def _():
        pl.semaphore_wait(hand.at[1], 1)

    for g in range(2):
        if g:
            query_half(1)
        part = query_group(g)
        for z in others:
            remote(qa.at[kv, part], 1, qrecv.at[g], {"kv": z, "tp": tp})

    turn(marks[0], marks[1])
    out_load.start()
    turn(marks[1], marks[2])
    for load in small_loads[1:]:
        load.wait()
    lane = lax.broadcasted_iota(jnp.int32, (rows, value_dim), 1)
    half = value_dim // 2
    first = lax.rem(lane, half) < half // 2
    cosines = table[0:1, :]
    sines = table[1:2, :]
    low = lax.broadcasted_iota(jnp.int32, (group, value_dim), 1) < half
    row_at = lax.broadcasted_iota(jnp.int32, (both, value_dim), 0)
    lane_at = lax.broadcasted_iota(jnp.int32, (both, value_dim), 1)

    def rotate_group(g, scale):
        for h in range(g * group, (g + 1) * group):
            total = qa[0, 1 + h]
            for z in range(1, kv_n):
                total = total + qa[z, 1 + h]
            total = total * scale
            swapped = jnp.where(
                first,
                pltpu.roll(total, value_dim - half // 2, 1),
                pltpu.roll(total, half // 2, 1),
            )
            qf[h] = total * cosines + swapped * sines

    def attend_group(g, beside):
        transpose(beside)
        spread = []
        for b in range(rows):
            query = qf[g * group:(g + 1) * group, b, :]
            grid = jnp.concatenate(
                [jnp.where(low, query, 0.0), jnp.where(low, 0.0, query)], axis=0
            ).astype(jnp.bfloat16)
            scores = inner_last(grid, kc[b]) * half ** (-0.5)
            peak = jnp.max(scores, axis=1, keepdims=True)
            exps = jnp.exp(scores - peak)
            sums = jnp.sum(exps, axis=1, keepdims=True)
            spread.append(exps.astype(jnp.bfloat16))
            stats = jnp.where(lane_at == row_at, peak, 0.0) + jnp.where(
                lane_at == row_at + both, sums, 0.0
            )
            st[kv, g, b:b + 1, :] = jnp.sum(stats, axis=0, keepdims=True)
        for b in range(rows):
            values = jnp.dot(spread[b], vc[b], preferred_element_type=jnp.float32)
            ms[g, b] = values
            mv[kv, g, b] = values.astype(jnp.bfloat16)
        for z in others:
            remote(st.at[kv, g], 2, srecv.at[g], {"kv": z, "tp": tp})
            remote(mv.at[kv, g], 3, mrecv.at[g], {"kv": z, "tp": tp})

    rest = pl.ds(0, kv_n - 1)
    arrived(qa.at[rest, query_group(0)], qrecv.at[0])
    square = qa[0, 0]
    for z in range(1, kv_n):
        square = square + qa[z, 0]
    scale = lax.rsqrt(square / (n_all * own) + EPS)
    rotate_group(0, scale)
    key_load.wait()
    value_load.wait()
    loaded(range(marks[2], marks[3]))
    attend_group(0, range(marks[2], marks[3]))
    arrived(qa.at[rest, query_group(1)], qrecv.at[1])
    rotate_group(1, scale)
    loaded(range(marks[3], marks[4]))
    attend_group(1, range(marks[3], marks[4]))

    for z in others:
        for side in range(tp_n):
            remote(tg.at[me], 0, trecv.at[1], {"kv": z, "tp": side})
    turn(marks[4], marks[5])
    out_load.wait()
    turn_out()
    lam_at = lax.broadcasted_iota(jnp.int32, (heads, heads), 0)
    lam_lane = lax.broadcasted_iota(jnp.int32, (heads, heads), 1)
    lam_col = jnp.sum(
        jnp.where(lam_at == lam_lane, lam[...], 0.0), axis=1, keepdims=True
    )
    sources = [kv] + others[::-1]

    def factor_group(g):
        signs = jnp.concatenate(
            [jnp.ones((group, 1), jnp.float32), -lam_col[g * group:(g + 1) * group]], axis=0
        )
        for b in range(rows):
            peaks, sums = [], []
            for z in sources:
                stats = st[z, g, b:b + 1, :]
                peaks.append(
                    jnp.sum(jnp.where(lane_at == row_at, stats, 0.0), axis=1, keepdims=True)
                )
                sums.append(
                    jnp.sum(
                        jnp.where(lane_at == row_at + both, stats, 0.0), axis=1, keepdims=True
                    )
                )
            top = peaks[0]
            for peak in peaks[1:]:
                top = jnp.maximum(top, peak)
            factors = [jnp.exp(peak - top) for peak in peaks]
            all_sums = jnp.zeros_like(top)
            for factor, total in zip(factors, sums):
                all_sums = all_sums + total * factor
            share = signs / all_sums
            for at, factor in enumerate(factors):
                cf[at, b] = jnp.broadcast_to(factor * share, (both, value_dim))

    def merge_group(g):
        for b in range(rows):
            weighted = ms[g, b] * cf[0, b]
            for at, z in enumerate(sources[1:]):
                weighted = weighted + mv[z, g, b].astype(jnp.float32) * cf[at + 1, b]
            difference = weighted[0:group] + weighted[group:both]
            norm = lax.rsqrt(jnp.mean(difference * difference, axis=1, keepdims=True) + EPS)
            hf[b] = difference * norm * hgain[...]
        return jnp.concatenate(
            [hf[:, h, :] for h in range(group)], axis=1
        ).astype(jnp.bfloat16)

    cut = features // 2
    for g in range(2):
        arrived(st.at[rest, g], srecv.at[g])
        factor_group(g)
        arrived(mv.at[rest, g], mrecv.at[g])
        flat = merge_group(g)
        if g == 0:
            loaded(range(marks[5], marks[6]))
            transpose(range(marks[5], marks[6]))
            oa[...] = jnp.dot(flat, wo_t[0:span, :], preferred_element_type=jnp.float32)
    near = others[::-1]
    loaded(range(marks[6], marks[7]))
    transpose(range(marks[6], marks[7]))
    part = jnp.dot(flat, wo_t[span:2 * span, :], preferred_element_type=jnp.float32)
    og[me] = (oa[...] + part).astype(jnp.bfloat16)
    remote(og.at[me], 4, orecv.at[kv], mate)
    for z in near:
        for side in range(tp_n):
            remote(og.at[me], 4, orecv.at[kv], {"kv": z, "tp": side})

    turn(marks[7], marks[8])
    arrived(tg.at[pl.ds(0, n_all - tp_n)], trecv.at[1])
    square = jnp.zeros((rows, 1), jnp.float32)
    for order, z in enumerate(sources):
        if order == 0:
            arrived(og.at[at_mate], orecv.at[kv])
        else:
            arrived(og.at[pl.ds(z * tp_n, tp_n)], orecv.at[z])
        tokens = jnp.concatenate(
            [tg[z * tp_n + side].astype(jnp.float32) for side in range(tp_n)], axis=1
        )
        attention = og[z * tp_n].astype(jnp.float32)
        for side in range(1, tp_n):
            attention = attention + og[z * tp_n + side].astype(jnp.float32)
        piece = tokens + attention
        at = pl.ds(pl.multiple_of(z * features, LANES), features)
        stream[:, at] = piece
        square = square + jnp.sum(piece * piece, axis=1, keepdims=True)
        gained = (piece * mgain[:, at]).astype(jnp.bfloat16)
        for g in range(2):
            product = jnp.dot(gained, wgu_t[g, at, :], preferred_element_type=jnp.float32)
            if order == 0:
                ga[g] = product
            else:
                ga[g] = ga[g] + product
    scale = lax.rsqrt(square / (n_all * own) + EPS)
    gate = ga[0] * scale
    up = ga[1] * scale
    hid[...] = (gate / (1.0 + jnp.exp(-gate)) * up).astype(jnp.bfloat16)
    hidden = hid[...]
    down_load.wait()

    def down_block(at):
        return jnp.dot(
            hidden,
            wd[:, pl.ds(pl.multiple_of(at * own, LANES), own)],
            preferred_element_type=jnp.float32,
        )

    targets = []
    for z in others:
        for side in range(tp_n):
            targets.append((z * tp_n + side, {"kv": z, "tp": side}))
    targets.append((at_mate, mate))
    pending = None

    def down_send(slot, block):
        at, where = targets[slot]
        ds[at] = block.astype(ds.dtype)
        remote(ds.at[at], 5, drecv.at[0], where, dr.at[me])

    for slot, (at, _) in enumerate(targets):
        block = down_block(at)
        if pending is not None:
            down_send(slot - 1, pending)
        pending = block
    total = down_block(me)
    down_send(len(targets) - 1, pending)
    total = total + stream[:, pl.ds(pl.multiple_of(me * own, LANES), own)]
    arrived(dr.at[pl.ds(0, n_all - 1)], drecv.at[0])
    total = total + dr[at_mate].astype(jnp.float32)
    for z in others[::-1]:
        for side in range(tp_n):
            total = total + dr[z * tp_n + side].astype(jnp.float32)
    out[...] = total.astype(out.dtype)
    apart = pl.ds(0, n_all - 1)
    for slot, ref in enumerate(
        [tg.at[apart], qa.at[rest], st.at[rest], mv.at[rest], og.at[apart], ds.at[apart]]
    ):
        batch(ref, sent.at[slot], sent.at[slot]).wait_send()


def turning(head_dim, position):
    half_len = head_dim // 4
    inv_freq = np.float32(1.0) / np.float32(THETA) ** (
        np.arange(half_len, dtype=np.float32) / np.float32(half_len)
    )
    angles = (np.float32(position) * inv_freq.astype(np.float32)).astype(np.float32)
    cos, sin = np.cos(angles), np.sin(angles)
    return np.stack(
        [np.concatenate([cos, cos] * 2), np.concatenate([-sin, sin] * 2)]
    ).astype(np.float32)


def fused(kv_n, tp_n, *arrays):
    (tokens, attn_gain, wq, kc, vc, lam, hgain, wo, mgain, wg, wu, wd) = arrays
    rows, own = tokens.shape
    n_all = kv_n * tp_n
    positions, value_dim = kc.shape[1], kc.shape[3]
    heads = lam.shape[0]
    model = n_all * own
    per_weight = wg.shape[0] // LANES
    slots = AHEAD + 2
    f32, bf16 = jnp.float32, jnp.bfloat16
    table = jnp.asarray(turning(value_dim, positions * kv_n))
    dma = pltpu.SemaphoreType.DMA
    hbm = pl.BlockSpec(memory_space=pl.ANY)
    return pl.pallas_call(
        functools.partial(fused_kernel, kv_n, tp_n),
        out_shape=pltpu.VMEM((rows, own), tokens.dtype),
        in_specs=[hbm] * 13,
        out_specs=pl.BlockSpec(memory_space=pltpu.VMEM),
        scratch_shapes=[
            pltpu.VMEM((1, model), f32),
            pltpu.VMEM((1, heads), f32),
            pltpu.VMEM((1, value_dim), f32),
            pltpu.VMEM((1, model), f32),
            pltpu.VMEM((2, value_dim), f32),
            pltpu.VMEM(wq.shape, bf16),
            pltpu.VMEM((rows, positions, value_dim), bf16),
            pltpu.VMEM((rows, positions, value_dim), bf16),
            pltpu.VMEM(wo.shape, bf16),
            pltpu.VMEM(wo.shape[::-1], bf16),
            pltpu.VMEM((slots, LANES, model), bf16),
            pltpu.VMEM((2,) + wg.shape[::-1], bf16),
            pltpu.VMEM(wd.shape, bf16),
            pltpu.VMEM((n_all, rows, own), bf16),
            pltpu.VMEM((kv_n, heads + 1, rows, value_dim), f32),
            pltpu.VMEM((heads, rows, value_dim), f32),
            pltpu.VMEM((2, rows, heads, value_dim), f32),
            pltpu.VMEM((kv_n, 2, rows, heads, value_dim), bf16),
            pltpu.VMEM((kv_n, 2, rows, value_dim), f32),
            pltpu.VMEM((kv_n, rows, heads, value_dim), f32),
            pltpu.VMEM((rows, heads // 2, value_dim), f32),
            pltpu.VMEM((rows, wo.shape[0]), f32),
            pltpu.VMEM((n_all, rows, wo.shape[0]), bf16),
            pltpu.VMEM((rows, model), f32),
            pltpu.VMEM((2, rows, wg.shape[0]), f32),
            pltpu.VMEM((rows, wg.shape[0]), bf16),
            pltpu.VMEM((n_all, rows, own), bf16),
            pltpu.VMEM((n_all, rows, own), bf16),
            pltpu.SemaphoreType.REGULAR((2,)),
            dma((6,)), dma((4,)), dma((slots,)), dma((6,)),
            dma((2,)), dma((2,)), dma((2,)), dma((2,)), dma((kv_n,)), dma((1,)),
        ],
        compiler_params=pltpu.CompilerParams(
            collective_id=0, has_side_effects=True, vmem_limit_bytes=65000000
        ),
    )(
        tokens, attn_gain.reshape(1, -1), wq,
        kc.reshape(rows, positions, value_dim), vc.reshape(rows, positions, value_dim),
        lam.reshape(1, -1), hgain.reshape(1, -1), wo, mgain.reshape(1, -1), wg, wu, wd, table,
    )


def layer(kv_n, tp_n, *arrays):
    tokens, kc, lam, wo, wg = arrays[0], arrays[3], arrays[5], arrays[7], arrays[9]
    units = wg.shape[0]
    small = tokens.shape[0] == kv_n and kc.shape[2] == 1 and tp_n == 2 and kv_n % 2 == 0
    whole = tokens.shape[1] % LANES == 0 and wo.shape[0] % (2 * LANES) == 0
    whole = whole and kc.shape[3] == LANES and lam.shape[0] % 2 == 0
    if small and whole and units % LANES == 0 and units % (8 * AHEAD) == 0:
        return fused(kv_n, tp_n, *arrays)
    return shards(*arrays)


def solution(mesh):
    placed = (
        P("dp", ("kv", "tp")),
        P(),
        P("kv", "tp"),
        P("dp", "kv", "tp", None),
        P("dp", "kv", "tp", None),
        P("tp"),
        P(),
        P("kv", "tp"),
        P(),
        P(("kv", "tp"), None),
        P(("kv", "tp"), None),
        P(("kv", "tp"), None),
    )
    return jax.shard_map(
        functools.partial(layer, mesh.shape["kv"], mesh.shape["tp"]),
        mesh=mesh, in_specs=placed, out_specs=P("dp", ("kv", "tp")), check_vma=False
    )
```

time: 28.3 us -> 25.8 us (0.912)
  Pallas kernels: 27.5 us -> 25 us
    pallas_call x1, Pallas kernels: 27.5 us -> 25 us  [fused(): pl.pallas_call(functools.partial(fused_kernel, kv_n, tp_n), out_shape=plt...]
where the time goes in v2:
time: 25.8 us; the launch traced here: 25.6 us
  Pallas kernels  25 us (97%)
  local copies, waits for them, and re-layouts  0.6 us (2%)
    pallas_call x1, Pallas kernels, fused(): pl.pallas_call(functools.partial(fused_kernel, kv_n, tp_n), out_shape=plt...  25 us
    unnamed x1, local copies, waits for them, and re-layouts  0.6 us

profile of v2, /device:TPU:0, one launch (start us, length us, event | category | flops | bytes accessed | tf_op | source)
XLA Modules:
  0.0 25.6 jit_solution(9143419069923720284)
XLA Ops:
  0.0 25.0 %shard_map.127 = bf16[4,512]{1,0:T(4,128)(2,1)S(1)} custom-call(bf16[4,512]{1,0:T(4,128)(2,1)} %tok_h.1, f32[1,4096]{1,0:T(1,128)} %bitcast.8, bf16[1024,2048]{1,0:T(8,128)(2,1)} %wq_h.1, bf16[4,256,128]{2,1,0:T(8,128)(2,1)} %bitcast.6, bf16[4,256,128]{2,1,0:T(8,128)(2,1)} %bitcast.7, f32[1,16]{1,0:T(1,128)} %bitcast.10, f32[1,128]{1,0:T(1,128)} %bitcast.11, ...), custom_call_target="tpu_custom_call" | custom-call | tf_op jit(solution)/shard_map/pallas_call | solution.py:601
  25.0 0.6 %copy.15 = bf16[4,512]{1,0:T(4,128)(2,1)} copy(bf16[4,512]{1,0:T(4,128)(2,1)S(1)} %shard_map.127) | data formatting | bytes 8192
